TPU v7x, 32 devices: a whole 2x2x4 slice. The times are simulated.
32 devices in a mesh: fs: 4 (over z), tp: 4 (over y, x), rep: 2 (over core).
Axes of the slice: x: 2, y: 2, z: 4, core: 2. Of those that a mesh axis runs over, the one named last changes fastest.
Arguments:
- up_weight: float32 [2048, 8192], P('fs', ('tp', 'rep')), may hold values from -0.125 to 0.125
- up_momentum: float32 [2048, 8192], P('fs', ('tp', 'rep')), may hold values from -24 to 24
- up_grads: bfloat16 [2, 2048, 8192], P('rep', 'fs', 'tp'), may hold values from -2.09375 to 2.09375
- out_weight: float32 [2048, 2048], P('fs', ('tp', 'rep')), may hold values from -0.125 to 0.125
- out_momentum: float32 [2048, 2048], P('fs', ('tp', 'rep')), may hold values from -24 to 24
- out_grads: bfloat16 [2, 2048, 2048], P('rep', 'fs', 'tp'), may hold values from -2.09375 to 2.09375
Outputs:
- up_weight_new: float32 [2048, 8192], P('fs', ('tp', 'rep'))
- up_momentum_new: float32 [2048, 8192], P('fs', ('tp', 'rep'))
- up_direction: float32 [2048, 8192], P('fs', ('tp', 'rep'))
- out_weight_new: float32 [2048, 2048], P('fs', ('tp', 'rep'))
- out_momentum_new: float32 [2048, 2048], P('fs', ('tp', 'rep'))
- out_direction: float32 [2048, 2048], P('fs', ('tp', 'rep'))
All inputs are finite; a program needn't handle non-finite values.
Results may differ from a plain program's by a relative error of at most 0.039.
Values may be sent and summed in bfloat16 or wider, within the bound.
No kernel may reach another device: no remote copies, remote signals or barrier semaphores. Data moves between devices by JAX's collectives and lax.ppermute only.
A program may use at most 64 MiB of HBM per device.

v0:
```python
import math
import jax
import jax.numpy as jnp
from jax import lax
from jax.sharding import PartitionSpec as P

ITERS = 3
MOMENT = 0.9
RATE = 0.02
COEF_A = 3.4445
COEF_B = -4.775
COEF_C = 2.0315


def local_gram(values, columns):
    return lax.dot_general(
        values, columns, (((1,), (1,)), ((), ())), preferred_element_type=jnp.float32
    )


def contract(gram, values, gram_axis):
    return lax.dot_general(
        gram, values, (((gram_axis,), (0,)), ((), ())), preferred_element_type=jnp.float32
    )


def second_product(gram, first_half, gram_axis):
    return contract(gram, lax.all_gather(first_half, "fs", axis=0, tiled=True), gram_axis)


def on_device(up_weight, up_momentum, up_grads, out_weight, out_momentum, out_grads):
    grad_up, grad_out = (
        lax.psum_scatter(
            up_grads[0].astype(jnp.float32).astype(jnp.bfloat16),
            "rep",
            scatter_dimension=1,
            tiled=True,
        ).astype(jnp.float32),
        lax.psum_scatter(
            out_grads[0].astype(jnp.float32).astype(jnp.bfloat16),
            "rep",
            scatter_dimension=1,
            tiled=True,
        ).astype(jnp.float32),
    )
    moments = [MOMENT * up_momentum + grad_up, MOMENT * out_momentum + grad_out]
    group = lax.axis_size("tp") * lax.axis_size("rep")
    current = moments
    for iteration in range(ITERS):
        values = [entry.astype(jnp.bfloat16) for entry in current]
        columns = (
            lax.all_gather(values[0], "fs", axis=0, tiled=True),
            lax.all_gather(values[1], "fs", axis=0, tiled=True),
        )
        gram_sums = (
            lax.psum(local_gram(values[0], columns[0]).astype(jnp.bfloat16), ("tp", "rep")).astype(
                jnp.float32
            ),
            lax.psum(local_gram(values[1], columns[1]).astype(jnp.bfloat16), ("tp", "rep")).astype(
                jnp.float32
            ),
        )
        gram_axis = 1
        if iteration == 0:
            totals = lax.psum(
                (jnp.sum(gram_sums[0] * gram_sums[0]), jnp.sum(gram_sums[1] * gram_sums[1])), "fs"
            )
        if iteration == 0:
            squares = [1.0 / (jnp.sqrt(total) + 1.0) for total in totals]
            factors = [jnp.sqrt(square) for square in squares]
        else:
            squares = [1.0, 1.0]
            factors = [1.0, 1.0]
        halves = [(gram_sums[index] * squares[index]).astype(jnp.bfloat16) for index in range(2)]
        products = [
            factors[index] * contract(halves[index], columns[index], gram_axis)
            for index in range(2)
        ]
        seconds = [
            second_product(halves[index], products[index].astype(jnp.bfloat16), gram_axis)
            for index in range(2)
        ]
        current = [
            COEF_A * factors[index] * current[index]
            + COEF_B * products[index]
            + COEF_C * seconds[index]
            for index in range(2)
        ]
    widths = [up_weight.shape[1] * group, out_weight.shape[1] * group]
    directions = [current[index] * math.sqrt(widths[index]) for index in range(2)]
    return (
        up_weight - RATE * directions[0],
        moments[0],
        directions[0],
        out_weight - RATE * directions[1],
        moments[1],
        directions[1],
    )


def solution(mesh):
    return jax.shard_map(
        on_device,
        mesh=mesh,
        in_specs=(
            P("fs", ("tp", "rep")),
            P("fs", ("tp", "rep")),
            P("rep", "fs", "tp"),
            P("fs", ("tp", "rep")),
            P("fs", ("tp", "rep")),
            P("rep", "fs", "tp"),
        ),
        out_specs=(
            P("fs", ("tp", "rep")),
            P("fs", ("tp", "rep")),
            P("fs", ("tp", "rep")),
            P("fs", ("tp", "rep")),
            P("fs", ("tp", "rep")),
            P("fs", ("tp", "rep")),
        ),
        check_vma=False,
    )
```

profile of v0, /device:TPU:0, one launch (start us, length us, event | category | flops | bytes accessed | tf_op | source)
XLA Modules:
  0.0 994.7 jit_solution(5314064352922162735)
XLA Ops:
  8.7 12.2 %reduce-scatter.5.cloned.1.call-done = bf16[512,256]{1,0:T(8,128)(2,1)} async-done(((bf16[512,512]{1,0:T(8,128)(2,1)}), bf16[512,256]{1,0:T(8,128)(2,1)}) %reduce-scatter.5.cloned.1.call-update) | async-done | bytes 262160 | tf_op jit(solution)/shard_map/reduce_scatter | solution.py:39
  22.9 11.0 %reduce-scatter.3.cloned.1.call-done = bf16[512,1024]{1,0:T(8,128)(2,1)} async-done(((bf16[512,2048]{1,0:T(8,128)(2,1)}), bf16[512,1024]{1,0:T(8,128)(2,1)}) %reduce-scatter.3.cloned.1.call-update) | async-done | bytes 1048592 | tf_op jit(solution)/shard_map/reduce_scatter | solution.py:33
  37.3 28.1 %all-gather.25.cloned.1.call-done = bf16[2048,256]{1,0:T(8,128)(2,1)} async-done(((bf16[512,256]{1,0:T(8,128)(2,1)}), bf16[2048,256]{1,0:T(8,128)(2,1)}) %all-gather.25.cloned.1.call-update) | async-done | bytes 1048592 | tf_op jit(solution)/shard_map/all_gather | solution.py:53
  68.7 78.9 %all-gather.13.cloned.1.call-done = bf16[2048,1024]{1,0:T(8,128)(2,1)} async-done(((bf16[512,1024]{1,0:T(8,128)(2,1)}), bf16[2048,1024]{1,0:T(8,128)(2,1)}) %all-gather.13.cloned.1.call-update) | async-done | bytes 4194320 | tf_op jit(solution)/shard_map/all_gather | solution.py:52
  153.5 79.4 %all-reduce.12.cloned.1.call-done = (bf16[512,2048]{1,0:T(8,128)(2,1)}, bf16[512,2048]{1,0:T(8,128)(2,1)}) async-done(((bf16[512,2048]{1,0:T(8,128)(2,1)}, bf16[512,2048]{1,0:T(8,128)(2,1)}), (bf16[512,2048]{1,0:T(8,128)(2,1)}, bf16[512,2048]{1,0:T(8,128)(2,1)})) %all-reduce.12.cloned.1.call-update) | async-done | bytes 4194320 | tf_op jit(solution)/shard_map/psum | solution.py:56
  236.9 12.3 %all-reduce = (f32[]{:T(128)}, f32[]{:T(128)}) all-reduce(f32[]{:T(128)} %get-tuple-element.42, f32[]{:T(128)} %get-tuple-element.43), channel_id=1, replica_groups=mesh['fs'=4,'tp'=4,'rep'=2] {'fs'}, use_global_device_ids=true, to_apply=%region_3.0 | all-reduce | flops 2 | bytes 16 | tf_op jit(solution)/shard_map/psum | solution.py:65
  254.2 6.3 multiply_convert_fusion
  260.6 18.3 %all-gather.27.cloned.1.call-done = bf16[2048,256]{1,0:T(8,128)(2,1)} async-done(((bf16[512,256]{1,0:T(8,128)(2,1)}), bf16[2048,256]{1,0:T(8,128)(2,1)}) %all-gather.27.cloned.1.call-update) | async-done | bytes 1048592 | tf_op jit(solution)/shard_map/all_gather | solution.py:28
  282.5 78.6 %all-gather.15.cloned.1.call-done = bf16[2048,1024]{1,0:T(8,128)(2,1)} async-done(((bf16[512,1024]{1,0:T(8,128)(2,1)}), bf16[2048,1024]{1,0:T(8,128)(2,1)}) %all-gather.15.cloned.1.call-update) | async-done | bytes 4194320 | tf_op jit(solution)/shard_map/all_gather | solution.py:28
  361.1 7.6 fusion.27
  369.0 20.8 %all-gather.29.cloned.1.call-done = bf16[2048,256]{1,0:T(8,128)(2,1)} async-done(((bf16[512,256]{1,0:T(8,128)(2,1)}), bf16[2048,256]{1,0:T(8,128)(2,1)}) %all-gather.29.cloned.1.call-update) | async-done | bytes 1048592 | tf_op jit(solution)/shard_map/all_gather | solution.py:53
  393.1 79.0 %all-gather.17.cloned.1.call-done = bf16[2048,1024]{1,0:T(8,128)(2,1)} async-done(((bf16[512,1024]{1,0:T(8,128)(2,1)}), bf16[2048,1024]{1,0:T(8,128)(2,1)}) %all-gather.17.cloned.1.call-update) | async-done | bytes 4194320 | tf_op jit(solution)/shard_map/all_gather | solution.py:52
  478.0 79.4 %all-reduce.10.cloned.1.call-done = (bf16[512,2048]{1,0:T(8,128)(2,1)}, bf16[512,2048]{1,0:T(8,128)(2,1)}) async-done(((bf16[512,2048]{1,0:T(8,128)(2,1)}, bf16[512,2048]{1,0:T(8,128)(2,1)}), (bf16[512,2048]{1,0:T(8,128)(2,1)}, bf16[512,2048]{1,0:T(8,128)(2,1)})) %all-reduce.10.cloned.1.call-update) | async-done | bytes 4194320 | tf_op jit(solution)/shard_map/psum | solution.py:56
  560.6 6.9 fusion.30
  567.6 21.1 %all-gather.31.cloned.1.call-done = bf16[2048,256]{1,0:T(8,128)(2,1)} async-done(((bf16[512,256]{1,0:T(8,128)(2,1)}), bf16[2048,256]{1,0:T(8,128)(2,1)}) %all-gather.31.cloned.1.call-update) | async-done | bytes 1048592 | tf_op jit(solution)/shard_map/all_gather | solution.py:28
  591.6 78.7 %all-gather.19.cloned.1.call-done = bf16[2048,1024]{1,0:T(8,128)(2,1)} async-done(((bf16[512,1024]{1,0:T(8,128)(2,1)}), bf16[2048,1024]{1,0:T(8,128)(2,1)}) %all-gather.19.cloned.1.call-update) | async-done | bytes 4194320 | tf_op jit(solution)/shard_map/all_gather | solution.py:28
  670.3 8.4 fusion.31
  678.7 20.2 %all-gather.33.cloned.1.call-done = bf16[2048,256]{1,0:T(8,128)(2,1)} async-done(((bf16[512,256]{1,0:T(8,128)(2,1)}), bf16[2048,256]{1,0:T(8,128)(2,1)}) %all-gather.33.cloned.1.call-update) | async-done | bytes 1048592 | tf_op jit(solution)/shard_map/all_gather | solution.py:53
  702.2 78.3 %all-gather.21.cloned.1.call-done = bf16[2048,1024]{1,0:T(8,128)(2,1)} async-done(((bf16[512,1024]{1,0:T(8,128)(2,1)}), bf16[2048,1024]{1,0:T(8,128)(2,1)}) %all-gather.21.cloned.1.call-update) | async-done | bytes 4194320 | tf_op jit(solution)/shard_map/all_gather | solution.py:52
  786.4 79.4 %all-reduce.8.cloned.1.call-done = (bf16[512,2048]{1,0:T(8,128)(2,1)}, bf16[512,2048]{1,0:T(8,128)(2,1)}) async-done(((bf16[512,2048]{1,0:T(8,128)(2,1)}, bf16[512,2048]{1,0:T(8,128)(2,1)}), (bf16[512,2048]{1,0:T(8,128)(2,1)}, bf16[512,2048]{1,0:T(8,128)(2,1)})) %all-reduce.8.cloned.1.call-update) | async-done | bytes 4194320 | tf_op jit(solution)/shard_map/psum | solution.py:56
  869.2 7.0 fusion.34
  876.2 20.9 %all-gather.35.cloned.1.call-done = bf16[2048,256]{1,0:T(8,128)(2,1)} async-done(((bf16[512,256]{1,0:T(8,128)(2,1)}), bf16[2048,256]{1,0:T(8,128)(2,1)}) %all-gather.35.cloned.1.call-update) | async-done | bytes 1048592 | tf_op jit(solution)/shard_map/all_gather | solution.py:28
  900.2 78.5 %all-gather.23.cloned.1.call-done = bf16[2048,1024]{1,0:T(8,128)(2,1)} async-done(((bf16[512,1024]{1,0:T(8,128)(2,1)}), bf16[2048,1024]{1,0:T(8,128)(2,1)}) %all-gather.23.cloned.1.call-update) | async-done | bytes 4194320 | tf_op jit(solution)/shard_map/all_gather | solution.py:28
  978.7 9.5 broadcast_multiply_fusion
  (83 shorter events, 58.3 us)
Async XLA Ops:
  7.2 13.7 %reduce-scatter.5.cloned.1.call-start = ((), (), s32[]{:S(2)}) async-start(), calls=%async_computation.9 | async-start | bytes 786432 | tf_op jit(solution)/shard_map/reduce_scatter | solution.py:39
  7.9 26.0 %reduce-scatter.3.cloned.1.call-start = ((), (), s32[]{:S(2)}) async-start(), calls=%async_computation.2 | async-start | bytes 3145728 | tf_op jit(solution)/shard_map/reduce_scatter | solution.py:33
  8.7 56.7 %all-gather.25.cloned.1.call-start = ((), (), s32[]{:S(2)}) async-start(), calls=%async_computation.10 | async-start | bytes 1310720 | tf_op jit(solution)/shard_map/all_gather | solution.py:53
  22.8 42.6 %copy-start.6 = (bf16[512,256]{1,0:T(8,128)(2,1)S(1)}, bf16[512,256]{1,0:T(8,128)(2,1)}, u32[]{:S(2)}) copy-start(bf16[512,256]{1,0:T(8,128)(2,1)} %get-tuple-element.14) | copy-start | bytes 786436
  22.8 124.7 %all-gather.13.cloned.1.call-start = ((), (), s32[]{:S(2)}) async-start(), calls=%async_computation.3 | async-start | bytes 5242880 | tf_op jit(solution)/shard_map/all_gather | solution.py:52
  37.2 110.3 %copy-start.4 = (bf16[512,1024]{1,0:T(8,128)(2,1)S(1)}, bf16[512,1024]{1,0:T(8,128)(2,1)}, u32[]{:S(2)}) copy-start(bf16[512,1024]{1,0:T(8,128)(2,1)} %get-tuple-element.16) | copy-start | bytes 3145732
  37.3 195.7 %all-reduce.12.cloned.1.call-start = ((), (), s32[]{:S(2)}) async-start(), calls=%async_computation.18 | async-start | bytes 8388608 | tf_op jit(solution)/shard_map/psum | solution.py:56
  153.4 125.4 %all-gather.27.cloned.1.call-start = ((), (), s32[]{:S(2)}) async-start(), calls=%async_computation.11 | async-start | bytes 1310720 | tf_op jit(solution)/shard_map/all_gather | solution.py:28
  253.4 107.8 %all-gather.15.cloned.1.call-start = ((), (), s32[]{:S(2)}) async-start(), calls=%async_computation.4 | async-start | bytes 5242880 | tf_op jit(solution)/shard_map/all_gather | solution.py:28
  260.5 129.3 %all-gather.29.cloned.1.call-start = ((), (), s32[]{:S(2)}) async-start(), calls=%async_computation.12 | async-start | bytes 1310720 | tf_op jit(solution)/shard_map/all_gather | solution.py:53
  278.8 82.3 %copy-start.8 = (f32[512,1024]{1,0:T(8,128)S(1)}, f32[512,1024]{1,0:T(8,128)}, u32[]{:S(2)}) copy-start(f32[512,1024]{1,0:T(8,128)} %get-tuple-element.17) | copy-start | bytes 6291460
  282.5 189.6 %all-gather.17.cloned.1.call-start = ((), (), s32[]{:S(2)}) async-start(), calls=%async_computation.5 | async-start | bytes 5242880 | tf_op jit(solution)/shard_map/all_gather | solution.py:52
  368.7 103.4 %copy-start.11 = (bf16[512,1024]{1,0:T(8,128)(2,1)S(1)}, bf16[512,1024]{1,0:T(8,128)(2,1)}, u32[]{:S(2)}) copy-start(bf16[512,1024]{1,0:T(8,128)(2,1)} %get-tuple-element.24) | copy-start | bytes 3145732
  368.7 188.7 %all-reduce.10.cloned.1.call-start = ((), (), s32[]{:S(2)}) async-start(), calls=%async_computation.17 | async-start | bytes 8388608 | tf_op jit(solution)/shard_map/psum | solution.py:56
  477.9 79.5 %copy-start.2 = (bf16[2048,256]{1,0:T(8,128)(2,1)S(1)}, bf16[2048,256]{1,0:T(8,128)(2,1)}, u32[]{:S(2)}) copy-start(bf16[2048,256]{1,0:T(8,128)(2,1)} %all-gather.29.cloned.1.call-done) | copy-start | bytes 3145732
  478.0 110.7 %all-gather.31.cloned.1.call-start = ((), (), s32[]{:S(2)}) async-start(), calls=%async_computation.13 | async-start | bytes 1310720 | tf_op jit(solution)/shard_map/all_gather | solution.py:28
  560.5 109.8 %all-gather.19.cloned.1.call-start = ((), (), s32[]{:S(2)}) async-start(), calls=%async_computation.6 | async-start | bytes 5242880 | tf_op jit(solution)/shard_map/all_gather | solution.py:28
  567.5 131.4 %all-gather.33.cloned.1.call-start = ((), (), s32[]{:S(2)}) async-start(), calls=%async_computation.14 | async-start | bytes 1310720 | tf_op jit(solution)/shard_map/all_gather | solution.py:53
  591.5 189.0 %all-gather.21.cloned.1.call-start = ((), (), s32[]{:S(2)}) async-start(), calls=%async_computation.7 | async-start | bytes 5242880 | tf_op jit(solution)/shard_map/all_gather | solution.py:52
  678.6 101.9 %copy-start.12 = (bf16[512,1024]{1,0:T(8,128)(2,1)S(1)}, bf16[512,1024]{1,0:T(8,128)(2,1)}, u32[]{:S(2)}) copy-start(bf16[512,1024]{1,0:T(8,128)(2,1)} %get-tuple-element.32) | copy-start | bytes 3145732
  678.6 187.2 %all-reduce.8.cloned.1.call-start = ((), (), s32[]{:S(2)}) async-start(), calls=%async_computation.16 | async-start | bytes 8388608 | tf_op jit(solution)/shard_map/psum | solution.py:56
  786.4 79.5 %copy-start.3 = (bf16[2048,256]{1,0:T(8,128)(2,1)S(1)}, bf16[2048,256]{1,0:T(8,128)(2,1)}, u32[]{:S(2)}) copy-start(bf16[2048,256]{1,0:T(8,128)(2,1)} %all-gather.33.cloned.1.call-done) | copy-start | bytes 3145732
  786.4 110.7 %all-gather.35.cloned.1.call-start = ((), (), s32[]{:S(2)}) async-start(), calls=%async_computation.15 | async-start | bytes 1310720 | tf_op jit(solution)/shard_map/all_gather | solution.py:28
  868.9 109.8 %all-gather.23.cloned.1.call-start = ((), (), s32[]{:S(2)}) async-start(), calls=%async_computation.8 | async-start | bytes 5242880 | tf_op jit(solution)/shard_map/all_gather | solution.py:28
  (10 other events, 223.7 us)
Sparse Core Ops, SparseCore 0:
  10.2 10.6 reduce-scatter.4
  23.1 10.7 reduce-scatter.2
  36.1 29.2 all-gather.24
  67.4 80.1 all-gather.12
  153.5 79.3 all-reduce.11
  253.5 25.3 all-gather.26
  281.0 80.1 all-gather.14
  363.3 26.4 all-gather.28
  391.9 80.1 all-gather.16
  478.1 79.3 all-reduce.9
  560.6 28.0 all-gather.30
  590.1 80.1 all-gather.18
  672.4 26.4 all-gather.32
  700.3 80.0 all-gather.20
  786.5 79.3 all-reduce.7
  869.0 28.0 all-gather.34
  898.5 80.1 all-gather.22
where the time goes:
time: 995 us
  waiting for transfers between devices  864 us (87%)
  matrix products  91.9 us (9%)
  between operations  15.6 us (2%)
  blocking collectives  12.3 us (1%)
    all_gather x6, waiting for transfers between devices, second_product(): lax.all_gather(first_half, 'fs', axis=0, tiled=True)  296 us
    psum x3, waiting for transfers between devices, on_device(): lax.psum(local_gram(values[0], columns[0]).astype(jnp.bfloat16), ('tp', '...  238 us
    all_gather x3, waiting for transfers between devices, on_device(): lax.all_gather(values[0], 'fs', axis=0, tiled=True)  236 us
    all_gather x3, waiting for transfers between devices, on_device(): lax.all_gather(values[1], 'fs', axis=0, tiled=True)  69.1 us
    dot_general x12, matrix products, contract(): lax.dot_general(gram, values, (((gram_axis,), (0,)), ((), ())), preferred...  64.4 us
    dot_general x6, matrix products, local_gram(): lax.dot_general(values, columns, (((1,), (1,)), ((), ())), preferred_elem...  27.5 us
  transfers between devices with their start and end apart: 17, of which 17 were waited for; matrix products, arithmetic and copies ran while one was open for 6% of the time, Pallas kernels for 0%

commit v1 on v0

--- a/solution.py
+++ b/solution.py
@@ -52,8 +52,9 @@
             lax.all_gather(values[0], "fs", axis=0, tiled=True),
             lax.all_gather(values[1], "fs", axis=0, tiled=True),
         )
+        _create_works = lambda frame: jnp.sum(jax.lax.all_gather(frame, ("tp", "rep")), axis=0)
         gram_sums = (
-            lax.psum(local_gram(values[0], columns[0]).astype(jnp.bfloat16), ("tp", "rep")).astype(
+            _create_works(local_gram(values[0], columns[0]).astype(jnp.bfloat16)).astype(
                 jnp.float32
             ),
             lax.psum(local_gram(values[1], columns[1]).astype(jnp.bfloat16), ("tp", "rep")).astype(

time: 995 us -> 1210 us (1.22)
  waiting for transfers between devices: 864 us -> 1040 us
  other arithmetic: 9.21 us -> 41.3 us
    all_gather x0 -> x3, waiting for transfers between devices: none -> 264 us  [on_device(): jax.lax.all_gather(frame, ('tp', 'rep'))]
    psum x3, waiting for transfers between devices: 238 us -> 173 us  [on_device(): lax.psum(local_gram(values[1], columns[1]).astype(jnp.bfloat16), ('tp', '...]
    reduce_sum x0 -> x4, other arithmetic: none -> 34.4 us  [the longest x3 31.1 us: on_device(): jnp.sum(jax.lax.all_gather(frame, ('tp', 'rep')), axis=0)]
    all_gather x6, waiting for transfers between devices: 296 us -> 279 us  [second_product(): lax.all_gather(first_half, 'fs', axis=0, tiled=True)]
  transfers between devices with their start and end apart: 17 -> 20, of which waited for: 17 -> 20; matrix products, arithmetic and copies ran while one was open for 6% -> 9% of each run, Pallas kernels for 0% -> 0%
where the time goes in v1:
time: 1210 us
  waiting for transfers between devices  1040 us (86%)
  matrix products  91.7 us (8%)
  other arithmetic  41.3 us (3%)
  between operations  16 us (1%)
  blocking collectives  12.3 us (1%)
    all_gather x6, waiting for transfers between devices, second_product(): lax.all_gather(first_half, 'fs', axis=0, tiled=True)  279 us
    all_gather x3, waiting for transfers between devices, on_device(): jax.lax.all_gather(frame, ('tp', 'rep'))  264 us
    all_gather x3, waiting for transfers between devices, on_device(): lax.all_gather(values[0], 'fs', axis=0, tiled=True)  236 us
    psum x3, waiting for transfers between devices, on_device(): lax.psum(local_gram(values[1], columns[1]).astype(jnp.bfloat16), ('tp', '...  173 us
    all_gather x3, waiting for transfers between devices, on_device(): lax.all_gather(values[1], 'fs', axis=0, tiled=True)  69 us
    dot_general x12, matrix products, contract(): lax.dot_general(gram, values, (((gram_axis,), (0,)), ((), ())), preferred...  64.1 us
    reduce_sum x3, other arithmetic, on_device(): jnp.sum(jax.lax.all_gather(frame, ('tp', 'rep')), axis=0)  31.1 us
    dot_general x6, matrix products, local_gram(): lax.dot_general(values, columns, (((1,), (1,)), ((), ())), preferred_elem...  27.6 us
  transfers between devices with their start and end apart: 20, of which 20 were waited for; matrix products, arithmetic and copies ran while one was open for 9% of the time, Pallas kernels for 0%

profile of v1, /device:TPU:0, one launch (start us, length us, event | category | flops | bytes accessed | tf_op | source)
XLA Modules:
  0.0 1207.5 jit_solution(7052504355610226510)
XLA Ops:
  8.7 12.2 %reduce-scatter.5.cloned.1.call-done = bf16[512,256]{1,0:T(8,128)(2,1)} async-done(((bf16[512,512]{1,0:T(8,128)(2,1)}), bf16[512,256]{1,0:T(8,128)(2,1)}) %reduce-scatter.5.cloned.1.call-update) | async-done | bytes 262160 | tf_op jit(solution)/shard_map/reduce_scatter | solution.py:39
  22.9 11.0 reduce-scatter.3.cloned.1.call-done
  37.3 28.1 %all-gather.31.cloned.1.call-done = bf16[2048,256]{1,0:T(8,128)(2,1)} async-done(((bf16[512,256]{1,0:T(8,128)(2,1)}), bf16[2048,256]{1,0:T(8,128)(2,1)}) %all-gather.31.cloned.1.call-update) | async-done | bytes 1048592 | tf_op jit(solution)/shard_map/all_gather | solution.py:53
  68.7 78.8 %all-gather.19.cloned.1.call-done = bf16[2048,1024]{1,0:T(8,128)(2,1)} async-done(((bf16[512,1024]{1,0:T(8,128)(2,1)}), bf16[2048,1024]{1,0:T(8,128)(2,1)}) %all-gather.19.cloned.1.call-update) | async-done | bytes 4194320 | tf_op jit(solution)/shard_map/all_gather | solution.py:52
  153.5 58.0 %all-reduce.5.cloned.1.call-done = bf16[512,2048]{1,0:T(8,128)(2,1)} async-done(((bf16[512,2048]{1,0:T(8,128)(2,1)}), bf16[512,2048]{1,0:T(8,128)(2,1)}) %all-reduce.5.cloned.1.call-update) | async-done | bytes 2097168 | tf_op jit(solution)/shard_map/psum | solution.py:60
  214.7 87.9 %all-gather.43.cloned.1.call-done = bf16[4096,2048]{1,0:T(8,128)(2,1)} async-done(((bf16[512,2048]{1,0:T(8,128)(2,1)}), bf16[4096,2048]{1,0:T(8,128)(2,1)}) %all-gather.43.cloned.1.call-update) | async-done | bytes 16777232 | tf_op jit(solution)/shard_map/all_gather | solution.py:55
  313.8 12.3 %all-reduce = (f32[]{:T(128)}, f32[]{:T(128)}) all-reduce(f32[]{:T(128)} %fusion, f32[]{:T(128)} %fusion.2), channel_id=1, replica_groups=mesh['fs'=4,'tp'=4,'rep'=2] {'fs'}, use_global_device_ids=true, to_apply=%region_3.0 | all-reduce | flops 2 | bytes 16 | tf_op jit(solution)/shard_map/psum | solution.py:66
  337.2 18.2 %all-gather.33.cloned.1.call-done = bf16[2048,256]{1,0:T(8,128)(2,1)} async-done(((bf16[512,256]{1,0:T(8,128)(2,1)}), bf16[2048,256]{1,0:T(8,128)(2,1)}) %all-gather.33.cloned.1.call-update) | async-done | bytes 1048592 | tf_op jit(solution)/shard_map/all_gather | solution.py:28
  359.0 78.8 %all-gather.21.cloned.1.call-done = bf16[2048,1024]{1,0:T(8,128)(2,1)} async-done(((bf16[512,1024]{1,0:T(8,128)(2,1)}), bf16[2048,1024]{1,0:T(8,128)(2,1)}) %all-gather.21.cloned.1.call-update) | async-done | bytes 4194320 | tf_op jit(solution)/shard_map/all_gather | solution.py:28
  445.5 20.8 %all-gather.35.cloned.1.call-done = bf16[2048,256]{1,0:T(8,128)(2,1)} async-done(((bf16[512,256]{1,0:T(8,128)(2,1)}), bf16[2048,256]{1,0:T(8,128)(2,1)}) %all-gather.35.cloned.1.call-update) | async-done | bytes 1048592 | tf_op jit(solution)/shard_map/all_gather | solution.py:53
  469.8 78.7 %all-gather.23.cloned.1.call-done = bf16[2048,1024]{1,0:T(8,128)(2,1)} async-done(((bf16[512,1024]{1,0:T(8,128)(2,1)}), bf16[2048,1024]{1,0:T(8,128)(2,1)}) %all-gather.23.cloned.1.call-update) | async-done | bytes 4194320 | tf_op jit(solution)/shard_map/all_gather | solution.py:52
  554.5 57.6 %all-reduce.7.cloned.1.call-done = bf16[512,2048]{1,0:T(8,128)(2,1)} async-done(((bf16[512,2048]{1,0:T(8,128)(2,1)}), bf16[512,2048]{1,0:T(8,128)(2,1)}) %all-reduce.7.cloned.1.call-update) | async-done | bytes 2097168 | tf_op jit(solution)/shard_map/psum | solution.py:60
  615.1 88.1 %all-gather.45.cloned.1.call-done = bf16[4096,2048]{1,0:T(8,128)(2,1)} async-done(((bf16[512,2048]{1,0:T(8,128)(2,1)}), bf16[4096,2048]{1,0:T(8,128)(2,1)}) %all-gather.45.cloned.1.call-update) | async-done | bytes 16777232 | tf_op jit(solution)/shard_map/all_gather | solution.py:55
  703.2 10.8 reduce_sum.56
  721.1 12.2 %all-gather.37.cloned.1.call-done = bf16[2048,256]{1,0:T(8,128)(2,1)} async-done(((bf16[512,256]{1,0:T(8,128)(2,1)}), bf16[2048,256]{1,0:T(8,128)(2,1)}) %all-gather.37.cloned.1.call-update) | async-done | bytes 1048592 | tf_op jit(solution)/shard_map/all_gather | solution.py:28
  736.2 78.7 %all-gather.25.cloned.1.call-done = bf16[2048,1024]{1,0:T(8,128)(2,1)} async-done(((bf16[512,1024]{1,0:T(8,128)(2,1)}), bf16[2048,1024]{1,0:T(8,128)(2,1)}) %all-gather.25.cloned.1.call-update) | async-done | bytes 4194320 | tf_op jit(solution)/shard_map/all_gather | solution.py:28
  823.3 20.1 %all-gather.39.cloned.1.call-done = bf16[2048,256]{1,0:T(8,128)(2,1)} async-done(((bf16[512,256]{1,0:T(8,128)(2,1)}), bf16[2048,256]{1,0:T(8,128)(2,1)}) %all-gather.39.cloned.1.call-update) | async-done | bytes 1048592 | tf_op jit(solution)/shard_map/all_gather | solution.py:53
  846.8 78.2 %all-gather.27.cloned.1.call-done = bf16[2048,1024]{1,0:T(8,128)(2,1)} async-done(((bf16[512,1024]{1,0:T(8,128)(2,1)}), bf16[2048,1024]{1,0:T(8,128)(2,1)}) %all-gather.27.cloned.1.call-update) | async-done | bytes 4194320 | tf_op jit(solution)/shard_map/all_gather | solution.py:52
  931.1 57.2 %all-reduce.9.cloned.1.call-done = bf16[512,2048]{1,0:T(8,128)(2,1)} async-done(((bf16[512,2048]{1,0:T(8,128)(2,1)}), bf16[512,2048]{1,0:T(8,128)(2,1)}) %all-reduce.9.cloned.1.call-update) | async-done | bytes 2097168 | tf_op jit(solution)/shard_map/psum | solution.py:60
  991.4 88.1 %all-gather.47.cloned.1.call-done = bf16[4096,2048]{1,0:T(8,128)(2,1)} async-done(((bf16[512,2048]{1,0:T(8,128)(2,1)}), bf16[4096,2048]{1,0:T(8,128)(2,1)}) %all-gather.47.cloned.1.call-update) | async-done | bytes 16777232 | tf_op jit(solution)/shard_map/all_gather | solution.py:55
  1079.5 10.8 reduce_sum.57
  1097.3 12.3 %all-gather.41.cloned.1.call-done = bf16[2048,256]{1,0:T(8,128)(2,1)} async-done(((bf16[512,256]{1,0:T(8,128)(2,1)}), bf16[2048,256]{1,0:T(8,128)(2,1)}) %all-gather.41.cloned.1.call-update) | async-done | bytes 1048592 | tf_op jit(solution)/shard_map/all_gather | solution.py:28
  1112.7 78.5 %all-gather.29.cloned.1.call-done = bf16[2048,1024]{1,0:T(8,128)(2,1)} async-done(((bf16[512,1024]{1,0:T(8,128)(2,1)}), bf16[2048,1024]{1,0:T(8,128)(2,1)}) %all-gather.29.cloned.1.call-update) | async-done | bytes 4194320 | tf_op jit(solution)/shard_map/all_gather | solution.py:28
  1191.2 9.5 broadcast_multiply_fusion
  (92 shorter events, 104.9 us)
Async XLA Ops:
  7.2 13.7 %reduce-scatter.5.cloned.1.call-start = ((), (), s32[]{:S(2)}) async-start(), calls=%async_computation.9 | async-start | bytes 786432 | tf_op jit(solution)/shard_map/reduce_scatter | solution.py:39
  7.9 26.0 %reduce-scatter.3.cloned.1.call-start = ((), (), s32[]{:S(2)}) async-start(), calls=%async_computation.2 | async-start | bytes 3145728 | tf_op jit(solution)/shard_map/reduce_scatter | solution.py:33
  8.7 56.7 %all-gather.31.cloned.1.call-start = ((), (), s32[]{:S(2)}) async-start(), calls=%async_computation.10 | async-start | bytes 1310720 | tf_op jit(solution)/shard_map/all_gather | solution.py:53
  22.8 124.7 %all-gather.19.cloned.1.call-start = ((), (), s32[]{:S(2)}) async-start(), calls=%async_computation.3 | async-start | bytes 5242880 | tf_op jit(solution)/shard_map/all_gather | solution.py:52
  37.3 110.3 %copy-start.4 = (bf16[512,1024]{1,0:T(8,128)(2,1)S(1)}, bf16[512,1024]{1,0:T(8,128)(2,1)}, u32[]{:S(2)}) copy-start(bf16[512,1024]{1,0:T(8,128)(2,1)} %get-tuple-element.10) | copy-start | bytes 3145732
  37.3 174.2 %all-reduce.5.cloned.1.call-start = ((), (), s32[]{:S(2)}) async-start(), calls=%async_computation.11 | async-start | bytes 4194304 | tf_op jit(solution)/shard_map/psum | solution.py:60
  68.7 233.9 %all-gather.43.cloned.1.call-start = ((), (), s32[]{:S(2)}) async-start(), calls=%async_computation.19 | async-start | bytes 18874368 | tf_op jit(solution)/shard_map/all_gather | solution.py:55
  153.4 202.0 %all-gather.33.cloned.1.call-start = ((), (), s32[]{:S(2)}) async-start(), calls=%async_computation.12 | async-start | bytes 1310720 | tf_op jit(solution)/shard_map/all_gather | solution.py:28
  330.0 107.7 %all-gather.21.cloned.1.call-start = ((), (), s32[]{:S(2)}) async-start(), calls=%async_computation.4 | async-start | bytes 5242880 | tf_op jit(solution)/shard_map/all_gather | solution.py:28
  337.2 129.2 %all-gather.35.cloned.1.call-start = ((), (), s32[]{:S(2)}) async-start(), calls=%async_computation.13 | async-start | bytes 1310720 | tf_op jit(solution)/shard_map/all_gather | solution.py:53
  358.9 189.6 %all-gather.23.cloned.1.call-start = ((), (), s32[]{:S(2)}) async-start(), calls=%async_computation.5 | async-start | bytes 5242880 | tf_op jit(solution)/shard_map/all_gather | solution.py:52
  445.3 103.2 %copy-start.9 = (bf16[512,1024]{1,0:T(8,128)(2,1)S(1)}, bf16[512,1024]{1,0:T(8,128)(2,1)}, u32[]{:S(2)}) copy-start(bf16[512,1024]{1,0:T(8,128)(2,1)} %get-tuple-element.18) | copy-start | bytes 3145732
  445.3 166.7 %all-reduce.7.cloned.1.call-start = ((), (), s32[]{:S(2)}) async-start(), calls=%async_computation.14 | async-start | bytes 4194304 | tf_op jit(solution)/shard_map/psum | solution.py:60
  469.7 233.4 %all-gather.45.cloned.1.call-start = ((), (), s32[]{:S(2)}) async-start(), calls=%async_computation.20 | async-start | bytes 18874368 | tf_op jit(solution)/shard_map/all_gather | solution.py:55
  554.4 57.6 %copy-start.2 = (bf16[2048,256]{1,0:T(8,128)(2,1)S(1)}, bf16[2048,256]{1,0:T(8,128)(2,1)}, u32[]{:S(2)}) copy-start(bf16[2048,256]{1,0:T(8,128)(2,1)} %all-gather.35.cloned.1.call-done) | copy-start | bytes 3145732
  554.4 178.9 %all-gather.37.cloned.1.call-start = ((), (), s32[]{:S(2)}) async-start(), calls=%async_computation.15 | async-start | bytes 1310720 | tf_op jit(solution)/shard_map/all_gather | solution.py:28
  615.0 199.8 %all-gather.25.cloned.1.call-start = ((), (), s32[]{:S(2)}) async-start(), calls=%async_computation.6 | async-start | bytes 5242880 | tf_op jit(solution)/shard_map/all_gather | solution.py:28
  721.0 122.4 %all-gather.39.cloned.1.call-start = ((), (), s32[]{:S(2)}) async-start(), calls=%async_computation.16 | async-start | bytes 1310720 | tf_op jit(solution)/shard_map/all_gather | solution.py:53
  736.1 188.8 %all-gather.27.cloned.1.call-start = ((), (), s32[]{:S(2)}) async-start(), calls=%async_computation.7 | async-start | bytes 5242880 | tf_op jit(solution)/shard_map/all_gather | solution.py:52
  823.3 101.7 %copy-start.10 = (bf16[512,1024]{1,0:T(8,128)(2,1)S(1)}, bf16[512,1024]{1,0:T(8,128)(2,1)}, u32[]{:S(2)}) copy-start(bf16[512,1024]{1,0:T(8,128)(2,1)} %get-tuple-element.22) | copy-start | bytes 3145732
  823.3 165.0 %all-reduce.9.cloned.1.call-start = ((), (), s32[]{:S(2)}) async-start(), calls=%async_computation.17 | async-start | bytes 4194304 | tf_op jit(solution)/shard_map/psum | solution.py:60
  846.7 232.7 %all-gather.47.cloned.1.call-start = ((), (), s32[]{:S(2)}) async-start(), calls=%async_computation.21 | async-start | bytes 18874368 | tf_op jit(solution)/shard_map/all_gather | solution.py:55
  930.9 178.8 %all-gather.41.cloned.1.call-start = ((), (), s32[]{:S(2)}) async-start(), calls=%async_computation.18 | async-start | bytes 1310720 | tf_op jit(solution)/shard_map/all_gather | solution.py:28
  991.3 199.8 %all-gather.29.cloned.1.call-start = ((), (), s32[]{:S(2)}) async-start(), calls=%async_computation.8 | async-start | bytes 5242880 | tf_op jit(solution)/shard_map/all_gather | solution.py:28
  (11 other events, 299.4 us)
Sparse Core Ops, SparseCore 0:
  10.2 10.6 reduce-scatter.4
  23.1 10.7 reduce-scatter.2
  36.1 29.2 all-gather.30
  67.4 80.1 all-gather.18
  151.2 60.2 all-reduce.4
  213.8 88.7 all-gather.42
  330.2 25.2 all-gather.32
  357.6 80.1 all-gather.20
  439.9 26.4 all-gather.34
  468.3 80.1 all-gather.22
  551.7 60.2 all-reduce.6
  614.3 88.7 all-gather.44
  705.3 27.9 all-gather.36
  734.7 80.1 all-gather.24
  816.9 26.4 all-gather.38
  844.8 80.1 all-gather.26
  928.0 60.2 all-reduce.8
  990.6 88.7 all-gather.46
  1081.6 27.9 all-gather.40
  1111.0 80.1 all-gather.28
